TPU v7x, 32 devices: a whole 2x2x4 slice. The times are simulated.
32 devices in a mesh: sp: 8 (over z, core), tp: 4 (over y, x).
Axes of the slice: x: 2, y: 2, z: 4, core: 2. Of those that a mesh axis runs over, the one named last changes fastest.
Arguments:
- query_heads: bfloat16 [2048, 1024], P('sp', 'tp'), may hold values from -6 to 6
- key_heads: bfloat16 [2048, 256], P('sp'), may hold values from -6 to 6
- value_heads: bfloat16 [2048, 256], P('sp'), may hold values from -24 to 24
- q_gain: float32 [64], replicated, may hold values from 0.6 to 4.5
- k_gain: float32 [64], replicated, may hold values from 0.6 to 4.5
- out_weight: bfloat16 [1024, 2048], P('tp'), may hold values from -0.1875 to 0.1875
- residual: bfloat16 [2048, 2048], P('sp', 'tp'), may hold values from -3 to 3
- norm_gain: float32 [2048], P('tp'), may hold values from 0.1 to 1.9
- routes: int32 [2048, 2], P('sp'), may hold values from 0 to 7, all different within a row; in each aligned block of 256 rows (0 to 255, 256 to 511, ...) at most 81 rows name the same one
- route_weights: float32 [2048, 2], P('sp'), may hold values from 0.5 to 1.5
- w_gate: bfloat16 [8, 2048, 4096], P('sp', None, 'tp'), may hold values from -0.125 to 0.125
- w_up: bfloat16 [8, 2048, 4096], P('sp', None, 'tp'), may hold values from -0.125 to 0.125
- w_down: bfloat16 [8, 4096, 2048], P('sp', 'tp'), may hold values from -0.1875 to 0.1875
Outputs:
- layer_out: bfloat16 [2048, 2048], P('sp', 'tp')
Inputs may be any that keep to these rules, and one draw needn't show every extreme that they name: `routes`: each row names 2 different experts. Among the 256 rows of one index of sp, no expert is named more than 81 times, a bound that some block reaches.
All inputs are finite; a program needn't handle non-finite values.
Results may differ from a plain program's by a relative error of at most 0.02.
The roundings to bfloat16 on the way count: a program that leaves them out, or rounds other values in their place, can miss the bound.
Values may be sent and summed in bfloat16 or wider, within the bound.
No kernel may reach another device: no remote copies, remote signals or barrier semaphores. Data moves between devices by JAX's collectives and lax.ppermute only.
A program may use at most 64 MiB of HBM per device.

v0:
```python
import jax
import jax.numpy as jnp
from jax import lax
from jax.sharding import PartitionSpec as P

D = 2048
HQ = 16
KV = 4
E = 64
TOPK = 2
GRID_W = 64
norm_eps = 1e-06
rope_base = 10000.0


def normalize(values_f, gain):
    mean_sq = jnp.mean(values_f * values_f, axis=-1, keepdims=True)
    return values_f * lax.rsqrt(mean_sq + norm_eps) * gain


def rotate(values_f, positions):
    head_width = values_f.shape[-1]
    half_width = head_width // 2
    quarter_width = half_width // 2
    frequency = rope_base ** (-jnp.arange(quarter_width, dtype=jnp.float32) / quarter_width)
    grid_rows = (positions // GRID_W).astype(jnp.float32)
    grid_cols = (positions % GRID_W).astype(jnp.float32)
    shape = (values_f.shape[0],) + (1,) * (values_f.ndim - 2) + (quarter_width,)
    pieces = []
    for coords, offset_lo in ((grid_rows, 0), (grid_cols, half_width)):
        angles = coords[:, None] * frequency[None, :]
        cosine = jnp.cos(angles).reshape(shape)
        sines = jnp.sin(angles).reshape(shape)
        first_part = values_f[..., offset_lo : offset_lo + quarter_width]
        second_part = values_f[..., offset_lo + quarter_width : offset_lo + half_width]
        pieces.append(first_part * cosine - second_part * sines)
        pieces.append(second_part * cosine + first_part * sines)
    return jnp.concatenate(pieces, axis=-1)


def shards(
    query_heads,
    key_heads,
    value_heads,
    q_gain,
    k_gain,
    out_weight,
    residual,
    norm_gain,
    routes,
    route_weights,
    w_gate,
    w_up,
    w_down,
):
    tok_rows = query_heads.shape[0]
    head_local = query_heads.shape[1] // E
    group_size = HQ // KV
    kv_count = max(head_local // group_size, 1)
    per_kv = head_local // kv_count
    tp_index = lax.axis_index("tp")
    sp_index = lax.axis_index("sp")
    kv_first = tp_index * head_local // group_size
    positions = sp_index * tok_rows + jnp.arange(tok_rows, dtype=jnp.int32)
    query_f = query_heads.astype(jnp.float32).reshape(tok_rows, kv_count, per_kv, E)
    q_turned = rotate(normalize(query_f, q_gain), positions).astype(jnp.bfloat16)
    key_cols = lax.dynamic_slice_in_dim(key_heads, kv_first * E, kv_count * E, 1)
    value_cols = lax.dynamic_slice_in_dim(value_heads, kv_first * E, kv_count * E, 1)
    key_f = key_cols.astype(jnp.float32).reshape(tok_rows, kv_count, E)
    k_turned = rotate(normalize(key_f, k_gain), positions).astype(jnp.bfloat16)
    value_sel = value_cols.reshape(tok_rows, kv_count, E)
    run_max = jnp.full((kv_count, per_kv, tok_rows), -1e30, jnp.float32)
    key_block = lax.all_gather(k_turned, "sp", axis=0, tiled=True)
    value_block = lax.all_gather(value_sel, "sp", axis=0, tiled=True)
    scores = jnp.einsum(
        "qcge,kce->cgqk", q_turned, key_block, preferred_element_type=jnp.float32
    ) * E ** (-0.5)
    new_max = jnp.maximum(run_max, jnp.max(scores, axis=-1))
    exped = jnp.exp(scores - new_max[..., None])
    denominator = jnp.sum(exped, axis=-1)
    weighted = jnp.einsum(
        "cgqk,kce->cgqe",
        exped.astype(jnp.bfloat16),
        value_block,
        preferred_element_type=jnp.float32,
    )
    run_max, denominator, weighted = (new_max, denominator, weighted)
    attended = (weighted / denominator[..., None]).astype(jnp.bfloat16)
    attended = attended.transpose(2, 0, 1, 3).reshape(tok_rows, head_local * E)
    partial_value = jnp.dot(attended, out_weight, preferred_element_type=jnp.float32).astype(
        jnp.bfloat16
    )
    attn_out = lax.psum_scatter(partial_value, "tp", scatter_dimension=1, tiled=True).astype(
        jnp.float32
    )
    after_attn = residual.astype(jnp.float32) + attn_out
    square_sum = lax.psum(jnp.sum(after_attn * after_attn, axis=1), "tp")
    normed = (after_attn * lax.rsqrt(square_sum / D + norm_eps)[:, None] * norm_gain).astype(
        jnp.bfloat16
    )
    experts_n = lax.axis_size("sp")
    capacity = 5 * tok_rows * TOPK // (4 * experts_n) + 1
    assign = routes.reshape(tok_rows * TOPK)
    onehot = (assign[:, None] == jnp.arange(experts_n, dtype=jnp.int32)[None, :]).astype(jnp.int32)
    before = jnp.cumsum(onehot, axis=0) - onehot
    slot_rank = jnp.sum(before * onehot, axis=1)
    slot_index = assign * capacity + slot_rank
    token_local = jnp.arange(tok_rows * TOPK, dtype=jnp.int32) // TOPK
    slot_token = (
        jnp.full((experts_n * capacity,), tok_rows, jnp.int32).at[slot_index].set(token_local)
    )
    gate_w = w_gate[0]
    up_w = w_up[0]
    down_w = w_down[0]
    padded = jnp.concatenate([normed, jnp.zeros((1, normed.shape[1]), jnp.bfloat16)], axis=0)
    slot_rows = padded[slot_token].reshape(experts_n, capacity, normed.shape[1])
    block_rows = lax.all_gather(
        lax.all_to_all(slot_rows, "sp", split_axis=0, concat_axis=0, tiled=True),
        "tp",
        axis=2,
        tiled=True,
    )
    gate_next = jnp.einsum("scd,df->scf", block_rows, gate_w, preferred_element_type=jnp.float32)
    up_next = jnp.einsum("scd,df->scf", block_rows, up_w, preferred_element_type=jnp.float32)
    activated = (jax.nn.silu(gate_next) * up_next).astype(jnp.bfloat16)
    partials = jnp.einsum(
        "scf,fd->scd", activated, down_w, preferred_element_type=jnp.float32
    ).astype(jnp.bfloat16)
    expert_rows = (
        lax.psum_scatter(partials, "tp", scatter_dimension=2, tiled=True)
        .astype(jnp.float32)
        .astype(jnp.bfloat16)
    )
    returned_rows = lax.all_to_all(expert_rows, "sp", split_axis=0, concat_axis=0, tiled=True)
    columns = returned_rows.shape[2]
    picked = returned_rows.reshape(experts_n * capacity, columns)[slot_index].astype(jnp.float32)
    picked = picked.reshape(tok_rows, TOPK, columns)
    expert_mix = jnp.sum(picked * route_weights[:, :, None], axis=1)
    return (after_attn + expert_mix).astype(jnp.bfloat16)


def solution(mesh):
    return jax.shard_map(
        shards,
        mesh=mesh,
        in_specs=(
            P("sp", "tp"),
            P("sp", None),
            P("sp", None),
            P(),
            P(),
            P("tp", None),
            P("sp", "tp"),
            P("tp"),
            P("sp", None),
            P("sp", None),
            P("sp", None, "tp"),
            P("sp", None, "tp"),
            P("sp", "tp", None),
        ),
        out_specs=P("sp", "tp"),
        check_vma=False,
    )
```

profile of v0, /device:TPU:0, one launch (start us, length us, event | category | flops | bytes accessed | tf_op | source)
XLA Modules:
  0.0 260.0 jit_solution(18293213865418719815)
XLA Ops:
  6.6 1.0 constant_dynamic-slice_fusion.1
  7.7 0.7 fusion.37
  8.9 15.9 %all_gather.9 = bf16[2048,1,64]{0,2,1:T(8,128)(2,1)S(1)} all-gather(bf16[256,1,64]{0,2,1:T(8,128)(2,1)S(1)} %pad_maximum_fusion), channel_id=1, replica_groups=mesh['sp'=8,'tp'=4] {'sp'}, dimensions={0}, use_global_device_ids=true | all-gather | bytes 294912 | tf_op jit(solution)/shard_map/all_gather | solution.py:73
  24.8 1.0 copy.20
  25.9 0.7 multiply_multiply_fusion
  26.7 4.5 %bitcast_reduce_fusion = (f32[4,256]{1,0:T(4,128)S(1)}, f32[2048,256,4]{1,0,2:T(8,128)}) fusion(bf16[256,4,16]{0,2,1:T(8,128)(2,1)S(1)} %get-tuple-element.9, bf16[256,4,16]{0,2,1:T(8,128)(2,1)S(1)} %get-tuple-element.10, bf16[256,4,16]{0,2,1:T(8,128)(2,1)S(1)} %get-tuple-element.6, bf16[256,4,16]{0,2,1:T(8,128)(2,1)S(1)} %get-tuple-element.5, ...), kind=kOutput, calls=%fused_computation.4 | convolution fusion | flops 273153024 | bytes 8785920 | tf_op jit(solution)/shard_map/qcge,kce->cgqk/dot_general | solution.py:75
  31.4 14.2 %all-gather = bf16[2048,64]{0,1:T(8,128)(2,1)S(1)} all-gather(bf16[256,64]{0,1:T(8,128)(2,1)S(1)} %copy.28), channel_id=2, replica_groups=mesh['sp'=8,'tp'=4] {'sp'}, dimensions={0}, use_global_device_ids=true | all-gather | bytes 294912 | tf_op jit(solution)/shard_map/all_gather | solution.py:74
  45.6 4.9 %fusion.1 = f32[4,256]{1,0:T(4,128)S(1)} fusion(f32[2048,256,4]{1,0,2:T(8,128)} %get-tuple-element.24, f32[4,256]{1,0:T(4,128)S(1)} %broadcast_maximum_fusion), kind=kLoop, calls=%fused_computation.6 | loop fusion | flops 6290432 | bytes 8396800 | tf_op jit(solution)/shard_map/reduce_sum | solution.py:80
  50.5 0.9 copy-done.1
  51.4 1.5 fusion.20
  52.9 1.5 convolution_convert_fusion
  54.9 1.1 reduce-window.6
  56.0 0.2 slice_reduce_fusion
  56.7 2.4 scatter_custom_fusion
  59.2 24.4 %reduce-scatter.3.cloned.1.call-done = bf16[256,512]{1,0:T(8,128)(2,1)} async-done(((bf16[256,2048]{1,0:T(8,128)(2,1)}), bf16[256,512]{1,0:T(8,128)(2,1)}) %reduce-scatter.3.cloned.1.call-update) | async-done | bytes 262160 | tf_op jit(solution)/shard_map/reduce_scatter | solution.py:93
  83.6 1.1 multiply_reduce_fusion.1
  84.7 8.9 %psum.7 = f32[256]{0:T(256)S(1)} all-reduce(f32[256]{0:T(256)S(1)} %multiply_reduce_fusion.1), channel_id=1, replica_groups=mesh['sp'=8,'tp'=4] {'tp'}, use_global_device_ids=true, to_apply=%region_6.7 | all-reduce | flops 256 | bytes 2048 | tf_op jit(solution)/shard_map/psum | solution.py:97
  93.7 1.1 multiply_convert_fusion.1
  94.8 2.8 %gather_fusion = bf16[648,512]{1,0:T(8,128)(2,1)S(1)} fusion(bf16[257,512]{1,0:T(8,128)(2,1)S(1)} %concatenate.36, s32[1024]{0:T(1024)S(1)} %pad_clamp_fusion.1), kind=kCustom, calls=%fused_computation | custom fusion | bytes 1329696 | tf_op jit(solution)/shard_map/gather | solution.py:116
  97.8 24.0 %all_to_all.10 = bf16[8,81,512]{2,1,0:T(8,128)(2,1)} all-to-all(bf16[8,81,512]{2,1,0:T(8,128)(2,1)S(1)} %reshape.562), channel_id=1, replica_groups=mesh['sp'=8,'tp'=4] {'sp'}, dimensions={0} | all-to-all | bytes 1327104 | tf_op jit(solution)/shard_map/all_to_all | solution.py:118
  121.9 0.2 reduce-scatter.5.cloned.1.call-start
  122.1 39.4 %all-gather.3.cloned.1.call-done = bf16[8,81,2048]{2,1,0:T(8,128)(2,1)} async-done(((bf16[8,81,512]{2,1,0:T(8,128)(2,1)}), bf16[8,81,2048]{2,1,0:T(8,128)(2,1)}) %all-gather.3.cloned.1.call-update) | async-done | bytes 2654224 | tf_op jit(solution)/shard_map/all_gather | solution.py:117
  161.5 7.8 %fusion.6 = f32[8,81,1024]{2,1,0:T(8,128)} fusion(bf16[8,81,2048]{2,1,0:T(8,128)(2,1)} %all-gather.3.cloned.1.call-done, bf16[1,2048,1024]{2,1,0:T(8,128)(2,1)} %param.24), kind=kOutput, calls=%fused_computation.11 | convolution fusion | flops 2717908992 | bytes 9502720 | tf_op jit(solution)/shard_map/scd,df->scf/dot_general | solution.py:124
  169.3 13.1 %fusion.12 = bf16[8,81,2048]{2,1,0:T(8,128)(2,1)} fusion(bf16[1,1024,2048]{2,1,0:T(8,128)(2,1)} %param.25, f32[8,81,1024]{2,1,0:T(8,128)} %fusion.6, bf16[8,81,2048]{2,1,0:T(8,128)(2,1)} %all-gather.3.cloned.1.call-done, bf16[1,2048,1024]{2,1,0:T(8,128)(2,1)} %param.23), kind=kOutput, calls=%fused_computation.16 | convolution fusion | flops 5441126400 | bytes 16351232 | tf_op jit(solution)/shard_map/scf,fd->scd/dot_general | solution.py:126
  182.4 41.9 %reduce-scatter.5.cloned.1.call-done = bf16[8,81,512]{2,1,0:T(8,128)(2,1)} async-done(((bf16[8,81,2048]{2,1,0:T(8,128)(2,1)}), bf16[8,81,512]{2,1,0:T(8,128)(2,1)}) %reduce-scatter.5.cloned.1.call-update) | async-done | bytes 663568 | tf_op jit(solution)/shard_map/reduce_scatter | solution.py:130
  224.3 4.6 %all-to-all-start.1 = ((bf16[8,81,512]{2,1,0:T(8,128)(2,1)}), bf16[8,81,512]{2,1,0:T(8,128)(2,1)S(1)}, u32[]{:S(2)}, u32[]{:S(2)}) async-start(bf16[8,81,512]{2,1,0:T(8,128)(2,1)} %reduce-scatter.5.cloned.1.call-done), calls=%async_computation.3 | async-start | bytes 1441792 | tf_op jit(solution)/shard_map/all_to_all | solution.py:134
  229.0 19.4 %all-to-all-done.1 = bf16[8,81,512]{2,1,0:T(8,128)(2,1)S(1)} async-done(((bf16[8,81,512]{2,1,0:T(8,128)(2,1)}), bf16[8,81,512]{2,1,0:T(8,128)(2,1)S(1)}, u32[]{:S(2)}, u32[]{:S(2)}) %all-to-all-start.1) | async-done | bytes 663584 | tf_op jit(solution)/shard_map/all_to_all | solution.py:134
  248.4 0.2 reshape.563
  248.6 2.0 gather_fusion.1
  250.6 0.7 reshape.566
  251.3 1.3 multiply_reduce_fusion
  252.6 0.8 add_convert_fusion
  (53 shorter events, 2.2 us)
Async XLA Ops:
  6.5 46.4 %copy-start = (bf16[256,2048]{1,0:T(8,128)(2,1)S(1)}, bf16[256,2048]{1,0:T(8,128)(2,1)}, u32[]{:S(2)}) copy-start(bf16[256,2048]{1,0:T(8,128)(2,1)} %param.18) | copy-start | bytes 3145732
  6.5 77.1 %reduce-scatter.3.cloned.1.call-start = ((), (), s32[]{:S(2)}) async-start(), calls=%async_computation.4 | async-start | bytes 1310720 | tf_op jit(solution)/shard_map/reduce_scatter | solution.py:93
  26.7 4.5 %copy-start.4 = (bf16[256,256]{1,0:T(8,128)(2,1)S(1)}, bf16[256,256]{1,0:T(8,128)(2,1)}, u32[]{:S(2)}) copy-start(bf16[256,256]{1,0:T(8,128)(2,1)} %param.15) | copy-start | bytes 393220
  45.6 5.8 %copy-start.1 = (f32[2048,256,4]{1,0,2:T(8,128)S(1)}, f32[2048,256,4]{1,0,2:T(8,128)}, u32[]{:S(2)}) copy-start(f32[2048,256,4]{1,0,2:T(8,128)} %get-tuple-element.24) | copy-start | bytes 25165828
  51.4 3.1 %copy-start.5 = (s32[256,2]{0,1:T(2,128)S(1)}, s32[256,2]{0,1:T(2,128)}, u32[]{:S(2)}) copy-start(s32[256,2]{0,1:T(2,128)} %param.21) | copy-start | bytes 6148
  52.9 30.7 %copy-start.2 = (bf16[256,512]{1,0:T(8,128)(2,1)S(1)}, bf16[256,512]{1,0:T(8,128)(2,1)}, u32[]{:S(2)}) copy-start(bf16[256,512]{1,0:T(8,128)(2,1)} %param.19) | copy-start | bytes 786436
  52.9 40.8 %copy-start.6 = (f32[512]{0:T(512)S(1)}, f32[512]{0:T(512)}, u32[]{:S(2)}) copy-start(f32[512]{0:T(512)} %param.20) | copy-start | bytes 6148
  54.4 107.1 %all-gather.3.cloned.1.call-start = ((), (), s32[]{:S(2)}) async-start(), calls=%async_computation.5 | async-start | bytes 3604480 | tf_op jit(solution)/shard_map/all_gather | solution.py:117
  121.9 102.4 %reduce-scatter.5.cloned.1.call-start = ((), (), s32[]{:S(2)}) async-start(), calls=%async_computation.6 | async-start | bytes 3604480 | tf_op jit(solution)/shard_map/reduce_scatter | solution.py:130
  182.4 46.5 %copy-start.7 = (f32[256,2]{0,1:T(2,128)S(1)}, f32[256,2]{0,1:T(2,128)}, u32[]{:S(2)}) copy-start(f32[256,2]{0,1:T(2,128)} %param.22) | copy-start | bytes 6148
  224.3 24.1 %all-to-all-start.1 = ((bf16[8,81,512]{2,1,0:T(8,128)(2,1)}), bf16[8,81,512]{2,1,0:T(8,128)(2,1)S(1)}, u32[]{:S(2)}, u32[]{:S(2)}) async-start(bf16[8,81,512]{2,1,0:T(8,128)(2,1)} %reduce-scatter.5.cloned.1.call-done), calls=%async_computation.3 | async-start | bytes 1441792 | tf_op jit(solution)/shard_map/all_to_all | solution.py:134
  248.6 4.0 %copy-start.3 = (bf16[256,512]{1,0:T(8,128)(2,1)S(1)}, bf16[256,512]{1,0:T(8,128)(2,1)}, u32[]{:S(2)}) copy-start(bf16[256,512]{1,0:T(8,128)(2,1)} %reduce-scatter.3.cloned.1.call-done) | copy-start | bytes 786436
Sparse Core Ops, SparseCore 0:
  54.5 29.0 reduce-scatter.2
  122.0 39.4 all-gather.2
  182.5 41.6 reduce-scatter.4
where the time goes:
time: 260 us
  waiting for transfers between devices  125 us (48%)
  blocking collectives  63.1 us (24%)
  matrix products  28.3 us (11%)
  between operations  13.4 us (5%)
  other arithmetic  12.6 us (5%)
  local copies, waits for them, and re-layouts  12.5 us (5%)
  starting transfers between devices  4.87 us (2%)
    reduce_scatter x1, waiting for transfers between devices, shards(): lax.psum_scatter(partials, 'tp', scatter_dimension=2, tiled=True)  41.9 us
    all_gather x1, waiting for transfers between devices, shards(): lax.all_gather(lax.all_to_all(slot_rows, 'sp', split_axis=0, concat_axis=...  39.4 us
    reduce_scatter x1, waiting for transfers between devices, shards(): lax.psum_scatter(partial_value, 'tp', scatter_dimension=1, tiled=True)  24.4 us
    all_to_all x1, blocking collectives, shards(): lax.all_to_all(slot_rows, 'sp', split_axis=0, concat_axis=0, tiled=True)  24 us
    all_to_all x1, waiting for transfers between devices, shards(): lax.all_to_all(expert_rows, 'sp', split_axis=0, concat_axis=0, tiled=True)  19.4 us
    all_gather x1, blocking collectives, shards(): key_block = lax.all_gather(k_turned, 'sp', axis=0, tiled=True)  15.9 us
    all_gather x1, blocking collectives, shards(): value_block = lax.all_gather(value_sel, 'sp', axis=0, tiled=True)  14.2 us
    dot_general x1, matrix products, shards(): jnp.einsum('scf,fd->scd', activated, down_w, preferred_element_type=jnp.f...  13.1 us
  transfers between devices with their start and end apart: 4, of which 4 were waited for; matrix products, arithmetic and copies ran while one was open for 2% of the time, Pallas kernels for 0%

commit v1 on v0

--- a/solution.py
+++ b/solution.py
@@ -70,8 +70,11 @@
     k_turned = rotate(normalize(key_f, k_gain), positions).astype(jnp.bfloat16)
     value_sel = value_cols.reshape(tok_rows, kv_count, E)
     run_max = jnp.full((kv_count, per_kv, tok_rows), -1e30, jnp.float32)
-    key_block = lax.all_gather(k_turned, "sp", axis=0, tiled=True)
-    value_block = lax.all_gather(value_sel, "sp", axis=0, tiled=True)
+    key_block, value_block = jnp.split(
+        lax.all_gather(jnp.concatenate([k_turned, value_sel], axis=1), "sp", axis=0, tiled=True),
+        [k_turned.shape[1]],
+        axis=1,
+    )
     scores = jnp.einsum(
         "qcge,kce->cgqk", q_turned, key_block, preferred_element_type=jnp.float32
     ) * E ** (-0.5)

time: 260 us -> 239 us (0.919)
  blocking collectives: 63.1 us -> 49.5 us
  other arithmetic: 12.6 us -> 9.04 us
  matrix products: 28.3 us -> 25.1 us
    all_gather x2 -> x1, blocking collectives: 30.1 us -> 16.5 us  [shards(): lax.all_gather(jnp.concatenate([k_turned, value_sel], axis=1), 'sp', axis...]
    reduce_sum x1, other arithmetic: 4.9 us -> 1.37 us  [shards(): denominator = jnp.sum(exped, axis=-1)]
    dot_general x1, matrix products: 4.51 us -> 1.29 us  [shards(): jnp.einsum('qcge,kce->cgqk', q_turned, key_block, preferred_element_type=...]
where the time goes in v1:
time: 239 us
  waiting for transfers between devices  125 us (52%)
  blocking collectives  49.5 us (21%)
  matrix products  25.1 us (11%)
  between operations  13.4 us (6%)
  local copies, waits for them, and re-layouts  11.6 us (5%)
  other arithmetic  9.04 us (4%)
  starting transfers between devices  4.87 us (2%)
    reduce_scatter x1, waiting for transfers between devices, shards(): lax.psum_scatter(partials, 'tp', scatter_dimension=2, tiled=True)  41.9 us
    all_gather x1, waiting for transfers between devices, shards(): lax.all_gather(lax.all_to_all(slot_rows, 'sp', split_axis=0, concat_axis=...  39.4 us
    reduce_scatter x1, waiting for transfers between devices, shards(): lax.psum_scatter(partial_value, 'tp', scatter_dimension=1, tiled=True)  24.4 us
    all_to_all x1, blocking collectives, shards(): lax.all_to_all(slot_rows, 'sp', split_axis=0, concat_axis=0, tiled=True)  24 us
    all_to_all x1, waiting for transfers between devices, shards(): lax.all_to_all(expert_rows, 'sp', split_axis=0, concat_axis=0, tiled=True)  19.4 us
    all_gather x1, blocking collectives, shards(): lax.all_gather(jnp.concatenate([k_turned, value_sel], axis=1), 'sp', axis...  16.5 us
    dot_general x1, matrix products, shards(): jnp.einsum('scf,fd->scd', activated, down_w, preferred_element_type=jnp.f...  13.1 us
    psum x1, blocking collectives, shards(): square_sum = lax.psum(jnp.sum(after_attn * after_attn, axis=1), 'tp')  8.96 us
  transfers between devices with their start and end apart: 4, of which 4 were waited for; matrix products, arithmetic and copies ran while one was open for 2% of the time, Pallas kernels for 0%

profile of v1, /device:TPU:0, one launch (start us, length us, event | category | flops | bytes accessed | tf_op | source)
XLA Modules:
  0.0 238.7 jit_solution(4513750402851621571)
XLA Ops:
  6.6 1.1 constant_dynamic-slice_fusion
  7.8 0.7 fusion.35
  8.7 0.2 fusion.53
  9.1 16.5 %all_gather.6 = bf16[2048,2,64]{0,2,1:T(8,128)(2,1)S(1)} all-gather(bf16[256,2,64]{0,2,1:T(8,128)(2,1)S(1)} %pad_maximum_fusion), channel_id=1, replica_groups=mesh['sp'=8,'tp'=4] {'sp'}, dimensions={0}, use_global_device_ids=true | all-gather | bytes 589824 | tf_op jit(solution)/shard_map/all_gather | solution.py:74
  25.6 1.0 copy.21
  26.6 0.7 multiply_multiply_fusion
  27.4 1.3 bitcast_reduce_fusion
  28.7 1.4 fusion.1
  30.1 1.5 fusion.20
  31.7 1.5 convolution_convert_fusion
  33.6 1.1 reduce-window.6
  34.8 0.2 slice_reduce_fusion
  35.5 2.4 %scatter_custom_fusion = s32[648]{0:T(1024)S(1)} fusion(s32[512]{0:T(512)S(1)} %bitcast.88, s32[512]{0:T(512)S(1)} %add_select_fusion, s32[]{:T(128)} %constant.96.clone.1), kind=kCustom, calls=%fused_computation.94 | custom fusion | bytes 2596 | tf_op jit(solution)/shard_map/scatter | solution.py:113
  37.9 24.4 %reduce-scatter.3.cloned.1.call-done = bf16[256,512]{1,0:T(8,128)(2,1)} async-done(((bf16[256,2048]{1,0:T(8,128)(2,1)}), bf16[256,512]{1,0:T(8,128)(2,1)}) %reduce-scatter.3.cloned.1.call-update) | async-done | bytes 262160 | tf_op jit(solution)/shard_map/reduce_scatter | solution.py:96
  62.3 1.1 multiply_reduce_fusion.1
  63.4 9.0 %psum.7 = f32[256]{0:T(256)S(1)} all-reduce(f32[256]{0:T(256)S(1)} %multiply_reduce_fusion.1), channel_id=1, replica_groups=mesh['sp'=8,'tp'=4] {'tp'}, use_global_device_ids=true, to_apply=%region_6.7 | all-reduce | flops 256 | bytes 2048 | tf_op jit(solution)/shard_map/psum | solution.py:100
  72.4 1.1 multiply_convert_fusion.1
  73.5 2.8 %gather_fusion = bf16[648,512]{1,0:T(8,128)(2,1)S(1)} fusion(bf16[257,512]{1,0:T(8,128)(2,1)S(1)} %concatenate.40, s32[1024]{0:T(1024)S(1)} %pad_clamp_fusion.1), kind=kCustom, calls=%fused_computation | custom fusion | bytes 1329696 | tf_op jit(solution)/shard_map/gather | solution.py:119
  76.3 0.2 reshape.562
  76.5 24.0 %all_to_all.10 = bf16[8,81,512]{2,1,0:T(8,128)(2,1)} all-to-all(bf16[8,81,512]{2,1,0:T(8,128)(2,1)S(1)} %reshape.562), channel_id=1, replica_groups=mesh['sp'=8,'tp'=4] {'sp'}, dimensions={0} | all-to-all | bytes 1327104 | tf_op jit(solution)/shard_map/all_to_all | solution.py:121
  100.6 0.2 reduce-scatter.5.cloned.1.call-start
  100.8 39.4 %all-gather.2.cloned.1.call-done = bf16[8,81,2048]{2,1,0:T(8,128)(2,1)} async-done(((bf16[8,81,512]{2,1,0:T(8,128)(2,1)}), bf16[8,81,2048]{2,1,0:T(8,128)(2,1)}) %all-gather.2.cloned.1.call-update) | async-done | bytes 2654224 | tf_op jit(solution)/shard_map/all_gather | solution.py:120
  140.2 7.8 %fusion.6 = f32[8,81,1024]{2,1,0:T(8,128)} fusion(bf16[8,81,2048]{2,1,0:T(8,128)(2,1)} %all-gather.2.cloned.1.call-done, bf16[1,2048,1024]{2,1,0:T(8,128)(2,1)} %param.24), kind=kOutput, calls=%fused_computation.11 | convolution fusion | flops 2717908992 | bytes 9502720 | tf_op jit(solution)/shard_map/scd,df->scf/dot_general | solution.py:127
  148.0 13.1 %fusion.12 = bf16[8,81,2048]{2,1,0:T(8,128)(2,1)} fusion(bf16[1,1024,2048]{2,1,0:T(8,128)(2,1)} %param.25, f32[8,81,1024]{2,1,0:T(8,128)} %fusion.6, bf16[8,81,2048]{2,1,0:T(8,128)(2,1)} %all-gather.2.cloned.1.call-done, bf16[1,2048,1024]{2,1,0:T(8,128)(2,1)} %param.23), kind=kOutput, calls=%fused_computation.16 | convolution fusion | flops 5441126400 | bytes 16351232 | tf_op jit(solution)/shard_map/scf,fd->scd/dot_general | solution.py:129
  161.1 41.9 %reduce-scatter.5.cloned.1.call-done = bf16[8,81,512]{2,1,0:T(8,128)(2,1)} async-done(((bf16[8,81,2048]{2,1,0:T(8,128)(2,1)}), bf16[8,81,512]{2,1,0:T(8,128)(2,1)}) %reduce-scatter.5.cloned.1.call-update) | async-done | bytes 663568 | tf_op jit(solution)/shard_map/reduce_scatter | solution.py:133
  203.0 4.6 %all-to-all-start.1 = ((bf16[8,81,512]{2,1,0:T(8,128)(2,1)}), bf16[8,81,512]{2,1,0:T(8,128)(2,1)S(1)}, u32[]{:S(2)}, u32[]{:S(2)}) async-start(bf16[8,81,512]{2,1,0:T(8,128)(2,1)} %reduce-scatter.5.cloned.1.call-done), calls=%async_computation.3 | async-start | bytes 1441792 | tf_op jit(solution)/shard_map/all_to_all | solution.py:137
  207.7 19.4 %all-to-all-done.1 = bf16[8,81,512]{2,1,0:T(8,128)(2,1)S(1)} async-done(((bf16[8,81,512]{2,1,0:T(8,128)(2,1)}), bf16[8,81,512]{2,1,0:T(8,128)(2,1)S(1)}, u32[]{:S(2)}, u32[]{:S(2)}) %all-to-all-start.1) | async-done | bytes 663584 | tf_op jit(solution)/shard_map/all_to_all | solution.py:137
  227.1 0.2 reshape.563
  227.3 2.0 gather_fusion.1
  229.3 0.7 reshape.566
  230.0 1.3 multiply_reduce_fusion
  231.3 0.8 add_convert_fusion
  (47 shorter events, 1.7 us)
Async XLA Ops:
  6.5 25.1 %copy-start = (bf16[256,2048]{1,0:T(8,128)(2,1)S(1)}, bf16[256,2048]{1,0:T(8,128)(2,1)}, u32[]{:S(2)}) copy-start(bf16[256,2048]{1,0:T(8,128)(2,1)} %param.18) | copy-start | bytes 3145732
  6.5 55.8 %reduce-scatter.3.cloned.1.call-start = ((), (), s32[]{:S(2)}) async-start(), calls=%async_computation.4 | async-start | bytes 1310720 | tf_op jit(solution)/shard_map/reduce_scatter | solution.py:96
  30.1 3.1 %copy-start.3 = (s32[256,2]{0,1:T(2,128)S(1)}, s32[256,2]{0,1:T(2,128)}, u32[]{:S(2)}) copy-start(s32[256,2]{0,1:T(2,128)} %param.21) | copy-start | bytes 6148
  31.6 30.7 %copy-start.1 = (bf16[256,512]{1,0:T(8,128)(2,1)S(1)}, bf16[256,512]{1,0:T(8,128)(2,1)}, u32[]{:S(2)}) copy-start(bf16[256,512]{1,0:T(8,128)(2,1)} %param.19) | copy-start | bytes 786436
  31.6 40.8 %copy-start.4 = (f32[512]{0:T(512)S(1)}, f32[512]{0:T(512)}, u32[]{:S(2)}) copy-start(f32[512]{0:T(512)} %param.20) | copy-start | bytes 6148
  33.1 107.1 %all-gather.2.cloned.1.call-start = ((), (), s32[]{:S(2)}) async-start(), calls=%async_computation.5 | async-start | bytes 3604480 | tf_op jit(solution)/shard_map/all_gather | solution.py:120
  100.6 102.4 %reduce-scatter.5.cloned.1.call-start = ((), (), s32[]{:S(2)}) async-start(), calls=%async_computation.6 | async-start | bytes 3604480 | tf_op jit(solution)/shard_map/reduce_scatter | solution.py:133
  161.1 46.5 %copy-start.5 = (f32[256,2]{0,1:T(2,128)S(1)}, f32[256,2]{0,1:T(2,128)}, u32[]{:S(2)}) copy-start(f32[256,2]{0,1:T(2,128)} %param.22) | copy-start | bytes 6148
  203.0 24.1 %all-to-all-start.1 = ((bf16[8,81,512]{2,1,0:T(8,128)(2,1)}), bf16[8,81,512]{2,1,0:T(8,128)(2,1)S(1)}, u32[]{:S(2)}, u32[]{:S(2)}) async-start(bf16[8,81,512]{2,1,0:T(8,128)(2,1)} %reduce-scatter.5.cloned.1.call-done), calls=%async_computation.3 | async-start | bytes 1441792 | tf_op jit(solution)/shard_map/all_to_all | solution.py:137
  227.3 4.0 %copy-start.2 = (bf16[256,512]{1,0:T(8,128)(2,1)S(1)}, bf16[256,512]{1,0:T(8,128)(2,1)}, u32[]{:S(2)}) copy-start(bf16[256,512]{1,0:T(8,128)(2,1)} %reduce-scatter.3.cloned.1.call-done) | copy-start | bytes 786436
Sparse Core Ops, SparseCore 0:
  33.3 29.0 reduce-scatter.2
  100.7 39.4 all-gather.1
  161.2 41.7 reduce-scatter.4
